TPU v7x, 256 devices: a whole 4x4x8 slice. The times are simulated.
256 devices in a mesh: sp: 32 (over z, y), tp: 8 (over x, core).
Axes of the slice: x: 4, y: 4, z: 8, core: 2. Of those that a mesh axis runs over, the one named last changes fastest.
Arguments:
- tokens: bfloat16 [4, 16384, 2048], P(None, ('sp', 'tp')), may hold values from -6 to 6
- in_gain: float32 [2048], replicated, may hold values from 0.1 to 1.9
- query_weight: bfloat16 [2048, 1024], P(None, 'tp'), may hold values from -0.125 to 0.125
- key_weight: bfloat16 [2048, 1024], P(None, 'tp'), may hold values from -0.125 to 0.125
- value_weight: bfloat16 [2048, 1024], P(None, 'tp'), may hold values from -0.125 to 0.125
- gate_weight: bfloat16 [2048, 1024], P(None, 'tp'), may hold values from -0.125 to 0.125
- log_decay: float32 [8], P('tp'), may hold values from -0.034 to 0, as said below
- norm_gain: float32 [1024], P('tp'), may hold values from 0.1 to 1.9
- out_weight: bfloat16 [1024, 2048], replicated, may hold values from -0.1875 to 0.1875
- post_gain: float32 [2048], replicated, may hold values from 0.1 to 1.9
Outputs:
- mixed: bfloat16 [4, 16384, 2048], P(None, ('sp', 'tp'))
Inputs may be any that keep to these rules, and one draw needn't show every extreme that they name: `log_decay`: every entry is negative; some heads keep a tenth or more of their memory over 16384 positions, others lose most of it within 30 to 100 positions.
All inputs are finite; a program needn't handle non-finite values.
Results may differ from a plain program's by a relative error of at most 0.015.
Values may be sent and summed in bfloat16 or wider, within the bound.
A program may use at most 64 MiB of HBM per device.

v0:
```python
import jax
import jax.numpy as jnp
from jax import lax
from jax.sharding import Mesh
from jax.sharding import PartitionSpec as P

HEAD_DIM = 128
BLOCK = 128
SP = ("sp_0", "sp_1")
SP_TP = ("sp_0", "sp_1", "tp")
rms_eps = 1e-06
group_eps = 1e-05
rope_base = 10000.0


def neutral_like(shard, identity):
    return jax.tree.map(
        lambda part, zero: jnp.zeros_like(part) + jnp.asarray(zero, part.dtype), shard, identity
    )


def entering(shard, axes, combine, identity):
    before = start = neutral_like(shard, identity)
    running = shard
    for axis in reversed(axes):
        length, mine = (lax.axis_size(axis), lax.axis_index(axis))
        pieces = jax.tree.map(lambda part: lax.all_gather(part, axis), running)
        inside, running = (start, start)
        for k in range(length):
            passed = k < mine
            running = combine(running, jax.tree.map(lambda part: part[k], pieces))
            inside = jax.tree.map(lambda new, old: jnp.where(passed, new, old), running, inside)
        before = combine(inside, before)
    return before


def rotate(values, positions):
    half_dim = values.shape[-1] // 2
    inverse = rope_base ** (-jnp.arange(half_dim, dtype=jnp.float32) / half_dim)
    angles = positions.astype(jnp.float32)[:, None] * inverse[None, :]
    cosine = jnp.cos(angles)
    sine_part = jnp.sin(angles)
    first_half = values[..., :half_dim].astype(jnp.float32)
    second = values[..., half_dim:].astype(jnp.float32)
    return jnp.concatenate(
        [first_half * cosine - second * sine_part, first_half * sine_part + second * cosine],
        axis=-1,
    )


def local_pass(queries, key_rows, values, log_decay):
    seq_count, head_count, length, head_width = queries.shape
    block_count = length // BLOCK
    offsets = jnp.arange(BLOCK, dtype=jnp.float32)
    distance = offsets[:, None] - offsets[None, :]
    rate_col = log_decay[:, None, None]
    inside = jnp.where(distance >= 0, jnp.exp(rate_col * jnp.maximum(distance, 0.0)), 0.0)
    query_scale = jnp.exp(log_decay[:, None] * (offsets + 1.0))[..., None]
    key_scale = jnp.exp(log_decay[:, None] * (BLOCK - 1.0 - offsets))[..., None]
    block_decay = jnp.exp(log_decay * BLOCK)[:, None, None]

    def to_blocks(arr):
        return arr.reshape(seq_count, head_count, block_count, BLOCK, arr.shape[-1]).transpose(
            2, 0, 1, 3, 4
        )

    def advance(memory, inputs):
        q_block, k_block, v_block = inputs
        scores = jnp.einsum("shqd,shkd->shqk", q_block, k_block, preferred_element_type=jnp.float32)
        weights = (scores * inside).astype(jnp.bfloat16)
        within = jnp.einsum("shqk,shkv->shqv", weights, v_block, preferred_element_type=jnp.float32)
        carried = jnp.einsum("shqd,shdv->shqv", q_block.astype(jnp.float32) * query_scale, memory)
        k_scaled = (k_block.astype(jnp.float32) * key_scale).astype(jnp.bfloat16)
        memory = memory * block_decay + jnp.einsum(
            "shkd,shkv->shdv", k_scaled, v_block, preferred_element_type=jnp.float32
        )
        return (memory, within + carried)

    start_memory = jnp.zeros((seq_count, head_count, head_width, values.shape[-1]), jnp.float32)
    end_state, outputs = lax.scan(
        advance, start_memory, (to_blocks(queries), to_blocks(key_rows), to_blocks(values))
    )
    outputs = outputs.transpose(1, 2, 0, 3, 4).reshape(
        seq_count, head_count, length, values.shape[-1]
    )
    return (outputs, end_state)


def combine(earlier, later_part):
    return (
        earlier[0] * later_part[0],
        earlier[1] * later_part[0][None, :, None, None] + later_part[1],
    )


def read_out(carried, queries, partial_out, log_decay):
    length = queries.shape[2]
    read_scale = jnp.exp(log_decay[:, None] * (jnp.arange(length, dtype=jnp.float32) + 1.0))[
        ..., None
    ]
    return partial_out + jnp.einsum(
        "shld,shdv->shlv", queries.astype(jnp.float32) * read_scale, carried
    )


def body(
    tokens,
    in_gain,
    query_weight,
    key_weight,
    value_weight,
    gate_weight,
    log_decay,
    norm_gain,
    out_weight,
    post_gain,
):
    seq_count, rows_dev, model_width = tokens.shape
    tp_size = lax.axis_size("tp")
    local_width = query_weight.shape[1]
    head_count = local_width // HEAD_DIM
    stretch = rows_dev * tp_size
    tok_f32 = tokens.astype(jnp.float32)
    normed = (
        tok_f32 * lax.rsqrt(jnp.mean(tok_f32 * tok_f32, axis=-1, keepdims=True) + rms_eps) * in_gain
    ).astype(jnp.bfloat16)
    joined = jnp.concatenate([query_weight, key_weight, value_weight, gate_weight], axis=1)
    projected = jnp.einsum(
        "kux,xt->kut",
        lax.all_gather(normed, "tp", axis=1, tiled=True),
        joined,
        preferred_element_type=jnp.float32,
    ).astype(jnp.bfloat16)

    def heads_of(columns):
        return columns.reshape(seq_count, stretch, head_count, HEAD_DIM).transpose(0, 2, 1, 3)

    positions = lax.axis_index(SP) * stretch + jnp.arange(stretch, dtype=jnp.int32)
    queries = rotate(heads_of(projected[..., :local_width]), positions).astype(jnp.bfloat16)
    key_rows = (
        rotate(heads_of(projected[..., local_width : 2 * local_width]), positions)
        * HEAD_DIM ** (-0.5)
    ).astype(jnp.bfloat16)
    values = heads_of(projected[..., 2 * local_width : 3 * local_width])
    gating = projected[..., 3 * local_width :]
    partial_out, end_state = local_pass(queries, key_rows, values, log_decay)
    span_decay = jnp.exp(log_decay * stretch)
    carried = entering(
        (span_decay, end_state), SP, combine, (jnp.ones_like(span_decay), jnp.zeros_like(end_state))
    )[1]
    retained = read_out(carried, queries, partial_out, log_decay)
    center = jnp.mean(retained, axis=-1, keepdims=True)
    spread = jnp.mean(jnp.square(retained - center), axis=-1, keepdims=True)
    normal = (
        ((retained - center) * lax.rsqrt(spread + group_eps))
        .transpose(0, 2, 1, 3)
        .reshape(seq_count, stretch, local_width)
    )
    gated = (normal * norm_gain * jax.nn.silu(gating.astype(jnp.float32))).astype(jnp.bfloat16)
    premix = jnp.einsum(
        "hor,rn->hon",
        lax.all_to_all(gated, "tp", split_axis=1, concat_axis=2, tiled=True),
        out_weight,
        preferred_element_type=jnp.float32,
    )
    mixed = (
        premix * lax.rsqrt(jnp.mean(premix * premix, axis=-1, keepdims=True) + rms_eps) * post_gain
    )
    return mixed.astype(jnp.bfloat16)


def solution(mesh):
    torus = Mesh(mesh.devices.reshape(8, 4, mesh.shape["tp"]), ("sp_0", "sp_1", "tp"))
    return jax.shard_map(
        body,
        mesh=torus,
        in_specs=(
            P(None, SP_TP, None),
            P(),
            P(None, "tp"),
            P(None, "tp"),
            P(None, "tp"),
            P(None, "tp"),
            P("tp"),
            P("tp"),
            P(),
            P(),
        ),
        out_specs=P(None, SP_TP, None),
        check_vma=False,
    )
```

profile of v0, /device:TPU:1, one launch (start us, length us, event | category | flops | bytes accessed | tf_op | source)
XLA Modules:
  0.0 204.7 jit_solution(9332395953188734523)
XLA Ops:
  6.5 1.6 fusion.44
  8.1 2.6 %fusion.46 = bf16[4,64,2048]{2,1,0:T(8,128)(2,1)} fusion(bf16[4,64,2048]{2,1,0:T(8,128)(2,1)} %param.12, f32[2048]{0:T(1024)} %param.13, f32[4,64]{1,0:T(4,128)S(1)} %add_rsqrt_fusion.2), kind=kLoop, calls=%fused_computation.48 | loop fusion | flops 2097152 | bytes 2106368 | tf_op jit(solution)/shard_map/convert_element_type | solution.py:126
  13.5 53.8 %all-gather.7.cloned.1.call-done = bf16[4,512,2048]{2,1,0:T(8,128)(2,1)} async-done(((bf16[4,64,2048]{2,1,0:T(8,128)(2,1)}), bf16[4,512,2048]{2,1,0:T(8,128)(2,1)}) %all-gather.7.cloned.1.call-update) | async-done | bytes 8388624 | tf_op jit(solution)/shard_map/all_gather | solution.py:130
  67.3 9.5 %fusion.54 = bf16[4,512,512]{1,2,0:T(8,128)(2,1)S(1)} fusion(bf16[4,512,2048]{2,1,0:T(8,128)(2,1)} %all-gather.7.cloned.1.call-done, bf16[2048,128]{0,1:T(8,128)(2,1)S(1)} %copy.42, bf16[2048,128]{0,1:T(8,128)(2,1)S(1)} %copy.41, bf16[2048,128]{0,1:T(8,128)(2,1)S(1)} %copy.40, bf16[2048,128]{0,1:T(8,128)(2,1)S(1)} %copy.39), kind=kOutput, calls=%fused_computation.59 | convolution fusion | flops 4304404480 | bytes 12582912 | tf_op jit(solution)/shard_map/kux,xt->kut/dot_general | solution.py:128
  76.9 1.0 slice_bitcast_fusion
  80.3 1.3 copy.44
  81.6 1.2 reshape_transpose_reshape.3
  83.5 0.9 copy-done.1
  84.8 11.9 %while.15 = (s32[]{:T(128)}, f32[4,1,128,128]{3,2,0,1:T(8,128)S(1)}, f32[4,4,1,128,128]{4,3,1,2,0:T(8,128)}, f32[1]{0:T(128)}, bf16[4,4,1,128,128]{4,3,1,2,0:T(8...) while((s32[]{:T(128)}, ...), condition=%wide.region_2.3_spmd.clone.clone.clone, body=%wide.region_1.2_spmd.clone.clone.clone.sunk | while | flops 67977728 | bytes 2496632 | solution.py:80
  84.8 0.7 select_bitcast_fusion.2
  86.5 0.9 fusion.147
  87.8 0.7 select_bitcast_fusion.2
  89.5 0.9 fusion.147
  90.8 0.7 select_bitcast_fusion.2
  92.5 0.9 fusion.147
  93.8 0.7 select_bitcast_fusion.2
  95.5 0.9 fusion.147
  96.8 0.7 copy-done
  98.8 8.4 %all-reduce = f32[4]{0:T(128)S(1)} all-reduce(f32[4]{0:T(128)S(1)} %exponential_dynamic-update-slice_fusion), channel_id=2, replica_groups=mesh['sp_0'=8,'sp_1'=4,'tp'=8] {'sp_1'}, use_global_device_ids=true, to_apply=%add | all-reduce | flops 4 | bytes 32
  107.2 0.7 slice_multiply_fusion.1
  107.9 1.3 slice_multiply_fusion
  109.9 12.2 %all-gather.11.cloned.1.call-done = f32[16,1,128,128]{3,2,1,0:T(8,128)} async-done(((f32[4,1,128,128]{3,2,1,0:T(8,128)}), f32[16,1,128,128]{3,2,1,0:T(8,128)}) %all-gather.11.cloned.1.call-update) | async-done | bytes 1048592 | tf_op jit(solution)/shard_map/all_gather | solution.py:27
  122.0 3.8 %slice_add_fusion.8 = f32[4,1,128,128]{3,2,1,0:T(8,128)} fusion(f32[16,1,128,128]{3,2,1,0:T(8,128)} %all-gather.11.cloned.1.call-done, f32[]{:T(128)} %bitcast.20, f32[]{:T(128)} %bitcast.18, f32[16,1,128,128]{3,2,0,1:T(8,128)} %bitcast.197, f32[]{:T(128)} %bitcast.16, f32[]{:T(128)} %bitcast.13), kind=kLoop, calls=%fused_computation.109 | loop fusion | flops 458752 | bytes 1310736 | tf_op jit(solution)/shard_map/add | solution.py:92
  126.4 1.3 dynamic-update-slice.1
  127.7 13.9 %all-reduce.1 = f32[8]{0:T(128)S(1)} all-reduce(f32[8]{0:T(128)S(1)} %dynamic-update-slice.1), channel_id=3, replica_groups=mesh['sp_0'=8,'sp_1'=4,'tp'=8] {'sp_0'}, use_global_device_ids=true, to_apply=%add.1 | all-reduce | flops 8 | bytes 64
  141.6 0.7 fusion.127
  146.3 18.7 %all-gather.9.cloned.1.call-done = f32[8,4,1,128,128]{4,3,2,1,0:T(8,128)} async-done(((f32[1,4,1,128,128]{4,3,2,1,0:T(8,128)}), f32[8,4,1,128,128]{4,3,2,1,0:T(8,128)}) %all-gather.9.cloned.1.call-update) | async-done | bytes 2097168 | tf_op jit(solution)/shard_map/all_gather | solution.py:27
  165.1 7.9 %fusion.128 = (f32[4,512]{1,0:T(4,128)S(1)}, f32[4,512,128]{1,2,0:T(8,128)S(1)}) fusion(f32[4,512,128]{1,2,0:T(8,128)S(1)} %reshape.499, f32[8,4,1,128,128]{4,3,1,2,0:T(8,128)} %bitcast.204, f32[4,1,128,128]{3,2,1,0:T(8,128)S(1)} %copy-done.4, f32[16,1,128,128]{3,2,0,1:T(8,128)S(1)} %bitcast.198, f32[16,1,128,128]{3,2,1,0:T(8,128)S(1)} %copy-done.3, ...), kind=kOutput, calls=%fused_computation.175 | convolution fusion | flops 71170048 | bytes 5777468 | tf_op jit(solution)/shard_map/shld,shdv->shlv/dot_general | solution.py:101
  173.2 1.5 fusion.62
  175.0 18.3 %all_to_all.18 = bf16[4,512,128]{2,0,1:T(4,128)(2,1)S(1)} all-to-all(bf16[4,512,128]{2,0,1:T(4,128)(2,1)S(1)} %copy.65), channel_id=1, replica_groups=mesh['sp_0'=8,'sp_1'=4,'tp'=8] {'tp'}, dimensions={1} | all-to-all | bytes 1048576 | tf_op jit(solution)/shard_map/all_to_all | solution.py:162
  193.4 3.6 %multiply_reduce_fusion = (f32[4,64]{1,0:T(4,128)S(1)}, f32[4,64,2048]{2,1,0:T(8,128)S(1)}) fusion(bf16[1024,2048]{1,0:T(8,128)(2,1)} %param.20, bf16[4,8,8,8,128]{4,3,2,1,0:T(8,128)(2,1)S(1)} %bitcast.203), kind=kOutput, calls=%fused_computation.58 | convolution fusion | flops 1074790144 | bytes 6816768 | tf_op jit(solution)/shard_map/hor,rn->hon/dot_general | solution.py:160
  197.0 1.2 multiply_convert_fusion.2
  (83 shorter events, 13.9 us)
Async XLA Ops:
  6.5 4.3 %copy-start.8 = (bf16[2048,128]{1,0:T(8,128)(2,1)S(1)}, bf16[2048,128]{1,0:T(8,128)(2,1)}, u32[]{:S(2)}) copy-start(bf16[2048,128]{1,0:T(8,128)(2,1)} %param.14) | copy-start | bytes 1572868
  6.5 60.8 %all-gather.7.cloned.1.call-start = ((), (), s32[]{:S(2)}) async-start(), calls=%async_computation.1 | async-start | bytes 9437184 | tf_op jit(solution)/shard_map/all_gather | solution.py:130
  8.1 3.0 %copy-start.9 = (bf16[2048,128]{1,0:T(8,128)(2,1)S(1)}, bf16[2048,128]{1,0:T(8,128)(2,1)}, u32[]{:S(2)}) copy-start(bf16[2048,128]{1,0:T(8,128)(2,1)} %param.15) | copy-start | bytes 1572868
  10.8 1.0 copy-start.10
  10.8 1.3 copy-start.11
  10.8 111.2 %all-gather.11.cloned.1.call-start = ((), (), s32[]{:S(2)}) async-start(), calls=%async_computation.3 | async-start | bytes 1310720 | tf_op jit(solution)/shard_map/all_gather | solution.py:27
  76.9 1.5 copy-start.2
  78.3 0.7 copy-start.6
  78.4 0.8 copy-start.7
  83.2 1.2 copy-start.1
  84.8 12.8 %copy-start.15 = (u32[256]{0:T(256)S(1)}, u32[256]{0:T(256)}, u32[]{:S(2)}) copy-start(u32[256]{0:T(256)} %constant.86) | copy-start | bytes 3076
  84.8 41.1 %copy-start.14 = (u32[256]{0:T(256)S(1)}, u32[256]{0:T(256)}, u32[]{:S(2)}) copy-start(u32[256]{0:T(256)} %constant.91) | copy-start | bytes 3076
  96.7 0.7 copy-start
  96.7 48.7 %copy-start.5 = (f32[4,4,1,128,128]{4,3,1,2,0:T(8,128)S(1)}, f32[4,4,1,128,128]{4,3,1,2,0:T(8,128)}, u32[]{:S(2)}) copy-start(f32[4,4,1,128,128]{4,3,1,2,0:T(8,128)} %get-tuple-element.58) | copy-start | bytes 3145732
  97.5 67.6 %all-gather.9.cloned.1.call-start = ((), (), s32[]{:S(2)}) async-start(), calls=%async_computation.2 | async-start | bytes 2359296 | tf_op jit(solution)/shard_map/all_gather | solution.py:27
  145.5 19.6 %copy-start.3 = (f32[16,1,128,128]{3,2,1,0:T(8,128)S(1)}, f32[16,1,128,128]{3,2,1,0:T(8,128)}, u32[]{:S(2)}) copy-start(f32[16,1,128,128]{3,2,1,0:T(8,128)} %all-gather.11.cloned.1.call-done) | copy-start | bytes 3145732
  145.5 19.6 %copy-start.4 = (f32[4,1,128,128]{3,2,1,0:T(8,128)S(1)}, f32[4,1,128,128]{3,2,1,0:T(8,128)}, u32[]{:S(2)}) copy-start(f32[4,1,128,128]{3,2,1,0:T(8,128)} %slice_add_fusion.8) | copy-start | bytes 786436
  165.1 8.1 %copy-start.13 = (f32[128]{0:T(128)S(1)}, f32[128]{0:T(128)}, u32[]{:S(2)}) copy-start(f32[128]{0:T(128)} %param.19) | copy-start | bytes 1540
  193.4 3.6 %copy-start.12 = (f32[2048]{0:T(1024)S(1)}, f32[2048]{0:T(1024)}, u32[]{:S(2)}) copy-start(f32[2048]{0:T(1024)} %param.21) | copy-start | bytes 24580
Sparse Core Ops, SparseCore 0:
  10.9 56.3 all-gather.6
  97.6 24.3 all-gather.10
  126.0 39.0 all-gather.8
where the time goes:
time: 205 us
  waiting for transfers between devices  84.8 us (41%)
  blocking collectives  40.6 us (20%)
  matrix products  27.4 us (13%)
  other arithmetic  20.4 us (10%)
  between operations  18 us (9%)
  local copies, waits for them, and re-layouts  13.3 us (6%)
    all_gather x1, waiting for transfers between devices, body(): lax.all_gather(normed, 'tp', axis=1, tiled=True)  53.8 us
    all_gather x2, waiting for transfers between devices, entering(): pieces = jax.tree.map(lambda part: lax.all_gather(part, axis), running)  30.9 us
    unnamed x2, blocking collectives  22.3 us
    all_to_all x1, blocking collectives, body(): lax.all_to_all(gated, 'tp', split_axis=1, concat_axis=2, tiled=True)  18.3 us
    dot_general x1, matrix products, body(): jnp.einsum('kux,xt->kut', lax.all_gather(normed, 'tp', axis=1, tiled=True...  9.51 us
    dot_general x1, matrix products, read_out(): jnp.einsum('shld,shdv->shlv', queries.astype(jnp.float32) * read_scale, c...  7.93 us
    unnamed x41, local copies, waits for them, and re-layouts  6.03 us
  transfers between devices with their start and end apart: 3, of which 3 were waited for; matrix products, arithmetic and copies ran while one was open for 4% of the time, Pallas kernels for 0%

commit v1 on v0

--- a/solution.py
+++ b/solution.py
@@ -127,7 +127,9 @@
     joined = jnp.concatenate([query_weight, key_weight, value_weight, gate_weight], axis=1)
     projected = jnp.einsum(
         "kux,xt->kut",
-        lax.all_gather(normed, "tp", axis=1, tiled=True),
+        jnp.concatenate(
+            lax.all_to_all(jnp.stack([normed] * lax.axis_size("tp")), "tp", 0, 0), axis=1
+        ),
         joined,
         preferred_element_type=jnp.float32,
     ).astype(jnp.bfloat16)

time: 205 us -> 263 us (1.28)
  waiting for transfers between devices: 84.8 us -> 123 us
  local copies, waits for them, and re-layouts: 13.3 us -> 26.1 us
  starting transfers between devices: 0.09 us -> 8.23 us
    all_to_all x0 -> x1, waiting for transfers between devices: none -> 91 us  [body(): lax.all_to_all(jnp.stack([normed] * lax.axis_size('tp')), 'tp', 0, 0)]
    all_gather x1 -> x0, waiting for transfers between devices: 53.8 us -> none  [body(): lax.all_gather(normed, 'tp', axis=1, tiled=True)]
    reshape x0 -> x1, local copies, waits for them, and re-layouts: none -> 8.28 us  [body(): jnp.concatenate(lax.all_to_all(jnp.stack([normed] * lax.axis_size('tp')),...]
    all_to_all x0 -> x1, starting transfers between devices: none -> 8.15 us  [body(): lax.all_to_all(jnp.stack([normed] * lax.axis_size('tp')), 'tp', 0, 0)]
    another operation x0 -> x1, local copies, waits for them, and re-layouts: none -> 4.3 us  [body(): jnp.stack([normed] * lax.axis_size('tp'))]
  transfers between devices with their start and end apart: 3 -> 3, of which waited for: 3 -> 3; matrix products, arithmetic and copies ran while one was open for 4% -> 3% of each run, Pallas kernels for 0% -> 0%
where the time goes in v1:
time: 263 us; the launch traced here: 262 us
  waiting for transfers between devices  123 us (47%)
  blocking collectives  39.5 us (15%)
  matrix products  27.4 us (10%)
  local copies, waits for them, and re-layouts  26.1 us (10%)
  other arithmetic  19.3 us (7%)
  between operations  18.3 us (7%)
  starting transfers between devices  8.23 us (3%)
    all_to_all x1, waiting for transfers between devices, body(): lax.all_to_all(jnp.stack([normed] * lax.axis_size('tp')), 'tp', 0, 0)  91 us
    all_gather x2, waiting for transfers between devices, entering(): pieces = jax.tree.map(lambda part: lax.all_gather(part, axis), running)  31.9 us
    unnamed x2, blocking collectives  20.9 us
    all_to_all x1, blocking collectives, body(): lax.all_to_all(gated, 'tp', split_axis=1, concat_axis=2, tiled=True)  18.7 us
    dot_general x1, matrix products, body(): jnp.einsum('kux,xt->kut', jnp.concatenate(lax.all_to_all(jnp.stack([norme...  9.51 us
    reshape x1, local copies, waits for them, and re-layouts, body(): jnp.concatenate(lax.all_to_all(jnp.stack([normed] * lax.axis_size('tp')),...  8.28 us
    all_to_all x1, starting transfers between devices, body(): lax.all_to_all(jnp.stack([normed] * lax.axis_size('tp')), 'tp', 0, 0)  8.15 us
    dot_general x1, matrix products, read_out(): jnp.einsum('shld,shdv->shlv', queries.astype(jnp.float32) * read_scale, c...  7.98 us
  transfers between devices with their start and end apart: 3, of which 3 were waited for; matrix products, arithmetic and copies ran while one was open for 3% of the time, Pallas kernels for 0%

profile of v1, /device:TPU:1, one launch (start us, length us, event | category | flops | bytes accessed | tf_op | source)
XLA Modules:
  0.0 262.0 jit_solution(14239087087213979959)
XLA Ops:
  6.5 1.5 fusion.44
  8.1 1.5 fusion.46
  9.6 4.3 %stack.2 = bf16[8,4,64,2048]{3,2,1,0:T(8,128)(2,1)} broadcast(bf16[4,64,2048]{2,1,0:T(8,128)(2,1)S(1)} %fusion.46), dimensions={1,2,3} | broadcast | bytes 9437184 | tf_op jit(solution)/shard_map/stack | solution.py:131
  13.9 8.2 %all-to-all-start = ((bf16[8,4,64,2048]{3,2,1,0:T(8,128)(2,1)}), bf16[8,4,64,2048]{3,2,1,0:T(8,128)(2,1)}, u32[]{:S(2)}, u32[]{:S(2)}) async-start(bf16[8,4,64,2048]{3,2,1,0:T(8,128)(2,1)} %stack.2), calls=%async_computation | async-start | bytes 16777216 | tf_op jit(solution)/shard_map/all_to_all | solution.py:131
  24.8 91.0 %all-to-all-done = bf16[8,4,64,2048]{3,2,1,0:T(8,128)(2,1)} async-done(((bf16[8,4,64,2048]{3,2,1,0:T(8,128)(2,1)}), bf16[8,4,64,2048]{3,2,1,0:T(8,128)(2,1)}, u32[]{:S(2)}, u32[]{:S(2)}) %all-to-all-start) | async-done | bytes 8388640 | tf_op jit(solution)/shard_map/all_to_all | solution.py:131
  115.8 8.3 %copy.39 = bf16[4,8,64,2048]{3,2,1,0:T(8,128)(2,1)} copy(bf16[4,8,64,2048]{3,2,0,1:T(8,128)(2,1)} %bitcast) | data formatting | bytes 16777216 | tf_op jit(solution)/shard_map/reshape | solution.py:130
  124.1 9.5 %fusion.54 = bf16[4,512,512]{1,2,0:T(8,128)(2,1)S(1)} fusion(bf16[4,512,2048]{2,1,0:T(8,128)(2,1)} %bitcast.198, bf16[2048,128]{0,1:T(8,128)(2,1)S(1)} %copy.43, bf16[2048,128]{0,1:T(8,128)(2,1)S(1)} %copy.42, bf16[2048,128]{0,1:T(8,128)(2,1)S(1)} %copy.41, bf16[2048,128]{0,1:T(8,128)(2,1)S(1)} %copy.40), kind=kOutput, calls=%fused_computation.59 | convolution fusion | flops 4304404480 | bytes 12582912 | tf_op jit(solution)/shard_map/kux,xt->kut/dot_general | solution.py:128
  133.6 1.0 slice_bitcast_fusion
  137.1 1.3 copy.45
  138.4 1.2 reshape_transpose_reshape.3
  140.3 0.9 copy-done.1
  141.6 11.9 %while.15 = (s32[]{:T(128)}, f32[4,1,128,128]{3,2,0,1:T(8,128)S(1)}, f32[4,4,1,128,128]{4,3,1,2,0:T(8,128)}, f32[1]{0:T(128)}, bf16[4,4,1,128,128]{4,3,1,2,0:T(8...) while((s32[]{:T(128)}, ...), condition=%wide.region_2.3_spmd.clone.clone.clone, body=%wide.region_1.2_spmd.clone.clone.clone.sunk | while | flops 67977728 | bytes 2496632 | solution.py:80
  141.6 0.7 select_bitcast_fusion.2
  143.3 0.9 fusion.147
  144.5 0.7 select_bitcast_fusion.2
  146.2 0.9 fusion.147
  149.2 0.9 fusion.147
  152.2 0.9 fusion.147
  153.5 0.7 copy-done
  154.9 0.7 exponential_dynamic-update-slice_fusion
  155.7 7.0 %all-reduce = f32[4]{0:T(128)S(1)} all-reduce(f32[4]{0:T(128)S(1)} %exponential_dynamic-update-slice_fusion), channel_id=2, replica_groups=mesh['sp_0'=8,'sp_1'=4,'tp'=8] {'sp_1'}, use_global_device_ids=true, to_apply=%add | all-reduce | flops 4 | bytes 32
  163.3 1.2 slice_multiply_fusion
  165.2 13.5 %all-gather.8.cloned.1.call-done = f32[16,1,128,128]{3,2,1,0:T(8,128)} async-done(((f32[4,1,128,128]{3,2,1,0:T(8,128)}), f32[16,1,128,128]{3,2,1,0:T(8,128)}) %all-gather.8.cloned.1.call-update) | async-done | bytes 1048592 | tf_op jit(solution)/shard_map/all_gather | solution.py:27
  178.7 3.9 %slice_add_fusion.8 = f32[4,1,128,128]{3,2,1,0:T(8,128)} fusion(f32[16,1,128,128]{3,2,1,0:T(8,128)} %all-gather.8.cloned.1.call-done, f32[]{:T(128)} %bitcast.22, f32[]{:T(128)} %bitcast.20, f32[16,1,128,128]{3,2,0,1:T(8,128)} %bitcast.200, f32[]{:T(128)} %bitcast.18, f32[]{:T(128)} %bitcast.15), kind=kLoop, calls=%fused_computation.109 | loop fusion | flops 458752 | bytes 1310736 | tf_op jit(solution)/shard_map/add | solution.py:92
  183.2 1.4 dynamic-update-slice.1
  184.5 13.9 %all-reduce.1 = f32[8]{0:T(128)S(1)} all-reduce(f32[8]{0:T(128)S(1)} %dynamic-update-slice.1), channel_id=3, replica_groups=mesh['sp_0'=8,'sp_1'=4,'tp'=8] {'sp_0'}, use_global_device_ids=true, to_apply=%add.1 | all-reduce | flops 8 | bytes 64
  203.1 18.4 %all-gather.6.cloned.1.call-done = f32[8,4,1,128,128]{4,3,2,1,0:T(8,128)} async-done(((f32[1,4,1,128,128]{4,3,2,1,0:T(8,128)}), f32[8,4,1,128,128]{4,3,2,1,0:T(8,128)}) %all-gather.6.cloned.1.call-update) | async-done | bytes 2097168 | tf_op jit(solution)/shard_map/all_gather | solution.py:27
  221.6 8.0 %fusion.128 = (f32[4,512]{1,0:T(4,128)S(1)}, f32[4,512,128]{1,2,0:T(8,128)S(1)}) fusion(f32[4,512,128]{1,2,0:T(8,128)S(1)} %reshape.509, f32[8,4,1,128,128]{4,3,1,2,0:T(8,128)} %bitcast.207, f32[4,1,128,128]{3,2,1,0:T(8,128)S(1)} %copy-done.4, f32[16,1,128,128]{3,2,0,1:T(8,128)S(1)} %bitcast.201, f32[16,1,128,128]{3,2,1,0:T(8,128)S(1)} %copy-done.3, ...), kind=kOutput, calls=%fused_computation.175 | convolution fusion | flops 71170048 | bytes 5777468 | tf_op jit(solution)/shard_map/shld,shdv->shlv/dot_general | solution.py:101
  229.8 1.5 fusion.62
  231.5 18.7 %all_to_all.23 = bf16[4,512,128]{2,0,1:T(4,128)(2,1)S(1)} all-to-all(bf16[4,512,128]{2,0,1:T(4,128)(2,1)S(1)} %copy.66), channel_id=1, replica_groups=mesh['sp_0'=8,'sp_1'=4,'tp'=8] {'tp'}, dimensions={1} | all-to-all | bytes 1048576 | tf_op jit(solution)/shard_map/all_to_all | solution.py:164
  250.3 3.6 %multiply_reduce_fusion = (f32[4,64]{1,0:T(4,128)S(1)}, f32[4,64,2048]{2,1,0:T(8,128)S(1)}) fusion(bf16[1024,2048]{1,0:T(8,128)(2,1)} %param.20, bf16[4,8,8,8,128]{4,3,2,1,0:T(8,128)(2,1)S(1)} %bitcast.206), kind=kOutput, calls=%fused_computation.58 | convolution fusion | flops 1074790144 | bytes 6816768 | tf_op jit(solution)/shard_map/hor,rn->hon/dot_general | solution.py:162
  253.9 1.2 multiply_convert_fusion.2
  (84 shorter events, 16.1 us)
Async XLA Ops:
  13.9 8.2 %copy-start.8 = (bf16[2048,128]{1,0:T(8,128)(2,1)S(1)}, bf16[2048,128]{1,0:T(8,128)(2,1)}, u32[]{:S(2)}) copy-start(bf16[2048,128]{1,0:T(8,128)(2,1)} %param.14) | copy-start | bytes 1572868
  13.9 8.5 %copy-start.9 = (bf16[2048,128]{1,0:T(8,128)(2,1)S(1)}, bf16[2048,128]{1,0:T(8,128)(2,1)}, u32[]{:S(2)}) copy-start(bf16[2048,128]{1,0:T(8,128)(2,1)} %param.15) | copy-start | bytes 1572868
  13.9 101.9 %all-to-all-start = ((bf16[8,4,64,2048]{3,2,1,0:T(8,128)(2,1)}), bf16[8,4,64,2048]{3,2,1,0:T(8,128)(2,1)}, u32[]{:S(2)}, u32[]{:S(2)}) async-start(bf16[8,4,64,2048]{3,2,1,0:T(8,128)(2,1)} %stack.2), calls=%async_computation | async-start | bytes 16777216 | tf_op jit(solution)/shard_map/all_to_all | solution.py:131
  22.1 1.0 copy-start.10
  22.1 1.3 copy-start.11
  22.1 156.6 %all-gather.8.cloned.1.call-start = ((), (), s32[]{:S(2)}) async-start(), calls=%async_computation.3 | async-start | bytes 1310720 | tf_op jit(solution)/shard_map/all_gather | solution.py:27
  133.6 1.5 copy-start.2
  135.1 0.7 copy-start.6
  135.1 0.8 copy-start.7
  140.0 1.2 copy-start.1
  141.5 12.8 %copy-start.15 = (u32[256]{0:T(256)S(1)}, u32[256]{0:T(256)}, u32[]{:S(2)}) copy-start(u32[256]{0:T(256)} %constant.86) | copy-start | bytes 3076
  141.5 41.0 %copy-start.14 = (u32[256]{0:T(256)S(1)}, u32[256]{0:T(256)}, u32[]{:S(2)}) copy-start(u32[256]{0:T(256)} %constant.91) | copy-start | bytes 3076
  153.5 0.7 copy-start
  153.5 48.8 %copy-start.5 = (f32[4,4,1,128,128]{4,3,1,2,0:T(8,128)S(1)}, f32[4,4,1,128,128]{4,3,1,2,0:T(8,128)}, u32[]{:S(2)}) copy-start(f32[4,4,1,128,128]{4,3,1,2,0:T(8,128)} %get-tuple-element.58) | copy-start | bytes 3145732
  154.2 67.3 %all-gather.6.cloned.1.call-start = ((), (), s32[]{:S(2)}) async-start(), calls=%async_computation.2 | async-start | bytes 2359296 | tf_op jit(solution)/shard_map/all_gather | solution.py:27
  202.3 19.3 %copy-start.3 = (f32[16,1,128,128]{3,2,1,0:T(8,128)S(1)}, f32[16,1,128,128]{3,2,1,0:T(8,128)}, u32[]{:S(2)}) copy-start(f32[16,1,128,128]{3,2,1,0:T(8,128)} %all-gather.8.cloned.1.call-done) | copy-start | bytes 3145732
  202.3 19.3 %copy-start.4 = (f32[4,1,128,128]{3,2,1,0:T(8,128)S(1)}, f32[4,1,128,128]{3,2,1,0:T(8,128)}, u32[]{:S(2)}) copy-start(f32[4,1,128,128]{3,2,1,0:T(8,128)} %slice_add_fusion.8) | copy-start | bytes 786436
  221.6 8.2 %copy-start.13 = (f32[128]{0:T(128)S(1)}, f32[128]{0:T(128)}, u32[]{:S(2)}) copy-start(f32[128]{0:T(128)} %param.19) | copy-start | bytes 1540
  250.3 3.6 %copy-start.12 = (f32[2048]{0:T(1024)S(1)}, f32[2048]{0:T(1024)}, u32[]{:S(2)}) copy-start(f32[2048]{0:T(1024)} %param.21) | copy-start | bytes 24580
Sparse Core Ops, SparseCore 0:
  154.3 24.2 all-gather.7
  182.7 38.8 all-gather.5
